TPU v7x, 1024 devices: a whole 8x8x8 slice. The times are simulated.
1024 devices in a mesh: tp: 1024 (over z, y, x, core).
Axes of the slice: x: 8, y: 8, z: 8, core: 2. Of those that a mesh axis runs over, the one named last changes fastest.
Arguments:
- tokens: bfloat16 [1024, 8, 128], P('tp'), may hold values from -6 to 6
- block_norm_gain: float32 [2, 4096], replicated, may hold values from 0.1 to 1.9
- receptance_weight: bfloat16 [2, 1024, 128, 64], P(None, 'tp'), may hold values from -0.09375 to 0.09375
- key_weight: bfloat16 [2, 1024, 128, 64], P(None, 'tp'), may hold values from -0.09375 to 0.09375
- value_weight: bfloat16 [2, 1024, 128, 64], P(None, 'tp'), may hold values from -0.09375 to 0.09375
- decay_weight: bfloat16 [2, 1024, 128, 64], P(None, 'tp'), may hold values from -0.09375 to 0.09375
- learning_rate_weight: bfloat16 [2, 1024, 128, 64], P(None, 'tp'), may hold values from -0.09375 to 0.09375
- gate_weight: bfloat16 [2, 1024, 128, 64], P(None, 'tp'), may hold values from -0.09375 to 0.09375
- decay_bias_fixed: float32 [2, 2048], replicated, may hold values from -5 to 2
- self_token_weight: float32 [2, 2048], replicated, may hold values from -1.5 to 1.5
- readout_norm_gain: float32 [2, 2048], replicated, may hold values from 0.1 to 1.9
- output_weight: bfloat16 [2, 1024, 64, 128], P(None, 'tp'), may hold values from -0.125 to 0.125
- state: float32 [2, 1024, 8, 4096], P(None, 'tp'), may hold values from -3 to 3
Outputs:
- mixed: bfloat16 [1024, 8, 128], P('tp')
- new_state: float32 [2, 1024, 8, 4096], P(None, 'tp')
All inputs are finite; a program needn't handle non-finite values.
Results may differ from a plain program's by a relative error of at most 0.018.
Values may be sent and summed in bfloat16 or wider, within the bound.
A program may use at most 32 MiB of HBM per device.

v0:
```python
import jax
import jax.numpy as jnp
from jax import lax
from jax.sharding import PartitionSpec as P

D = 4096


RMS_EPS = 1e-06
GROUP_EPS = 0.00064


def swapped(shard, axis, stride):
    return lax.ppermute(shard, axis, [(i, i ^ 1 << stride) for i in range(lax.axis_size(axis))])


def for_sending(shard):

    def short(part):
        return part.astype(jnp.bfloat16) if part.dtype == jnp.float32 else part

    return jax.tree.map(short, shard)


def recurrent_update(
    layer_state,
    receptance_vector,
    key_vector,
    value_vector,
    decay_logits,
    learning_rate_logits,
    gate_logits,
    decay_constant,
    self_term_scale,
    head_gain_slice,
):
    highest = lax.Precision.HIGHEST
    shrink = jnp.exp(-jnp.exp(-jax.nn.softplus(-(decay_constant + decay_logits)) - 0.5))
    rate = jax.nn.sigmoid(learning_rate_logits)
    normed = key_vector * lax.rsqrt(jnp.sum(key_vector * key_vector, -1, keepdims=True) + 1.0)
    removed = jnp.einsum("...ij,...j->...i", layer_state, normed, precision=highest)
    layer_state = (
        layer_state * shrink[..., None, :]
        - removed[..., :, None] * (normed * rate)[..., None, :]
        + value_vector[..., :, None] * (key_vector * rate)[..., None, :]
    )
    readout = jnp.einsum("...ij,...j->...i", layer_state, receptance_vector, precision=highest)
    center = jnp.mean(readout, -1, keepdims=True)
    spread = jnp.mean(jnp.square(readout - center), -1, keepdims=True)
    normed_output = (readout - center) * lax.rsqrt(spread + GROUP_EPS) * head_gain_slice
    self_term = (
        jnp.sum(receptance_vector * key_vector * self_term_scale, -1, keepdims=True) * value_vector
    )
    return (
        ((normed_output + self_term) * jax.nn.sigmoid(gate_logits)).astype(jnp.bfloat16),
        layer_state,
    )


def double_gather(piece, position, first_bit, count, mover):
    for offset in range(count):
        which_bit = first_bit + offset
        partner = mover(piece, which_bit)
        lower_self = position >> which_bit & 1 == 0
        piece = jnp.where(
            lower_self, jnp.concatenate([piece, partner], 0), jnp.concatenate([partner, piece], 0)
        )
    return piece


def double_sum(total, first_bit, count, mover):
    for offset in range(count):
        total = total + mover(total, first_bit + offset)
    return total


def halve_sum(members, position, first_bit, count, mover):
    for offset in reversed(range(count)):
        which_bit = first_bit + offset
        upper_self = position >> which_bit & 1 == 1
        sends = tuple(
            (
                jnp.where(
                    upper_self, member[: member.shape[0] // 2], member[member.shape[0] // 2 :]
                )
                for member in members
            )
        )
        keeps = tuple(
            (
                jnp.where(
                    upper_self, member[member.shape[0] // 2 :], member[: member.shape[0] // 2]
                )
                for member in members
            )
        )
        arrived = mover(sends, which_bit)
        members = tuple((kept + got for kept, got in zip(keeps, arrived)))
    return members


def on_device(
    tokens,
    block_norm_gain,
    receptance_weight,
    key_weight,
    value_weight,
    decay_weight,
    learning_rate_weight,
    gate_weight,
    decay_bias_fixed,
    self_token_weight,
    readout_norm_gain,
    output_weight,
    state,
):
    columns_dev = tokens.shape[2]
    row_blocks = D // columns_dev
    low_bits = row_blocks.bit_length() - 1
    head_count = lax.axis_size("tp") // row_blocks
    high_bits = head_count.bit_length() - 1
    position = lax.axis_index("tp")
    head_index = position // row_blocks
    row_block = position % row_blocks
    head_size = receptance_weight.shape[3]
    seq_tile = tokens.shape[1]
    move_rows = lambda payload, which_bit: swapped(payload, "tp", which_bit)
    move_proj = lambda payload, which_bit: swapped(payload, "tp", which_bit)
    move_outs = lambda payload, which_bit: swapped(payload, "tp", which_bit)
    move_split = lambda payload, which_bit: jax.tree.map(
        lambda part, own: part.astype(own.dtype),
        swapped(for_sending(payload), "tp", which_bit),
        payload,
    )

    def mixer(columns, layer_index):
        gain_cols = lax.dynamic_slice_in_dim(
            block_norm_gain[layer_index], row_block * columns_dev, columns_dev
        )
        wide = columns.astype(jnp.float32)
        scaled = (wide * gain_cols).astype(jnp.bfloat16)
        squares = jnp.sum(wide * wide, axis=1)
        weights = jnp.concatenate(
            [
                receptance_weight[layer_index, 0],
                key_weight[layer_index, 0],
                value_weight[layer_index, 0],
                decay_weight[layer_index, 0],
                learning_rate_weight[layer_index, 0],
                gate_weight[layer_index, 0],
            ],
            axis=1,
        )
        partial_value = jnp.dot(scaled, weights, preferred_element_type=jnp.float32)
        summed, total_sq = halve_sum((partial_value, squares), position, 0, low_bits, move_proj)
        projected = summed * lax.rsqrt(total_sq / D + RMS_EPS)[:, None]
        output_pieces = jnp.split(projected, 6, axis=1)

        def head_columns(table):
            return lax.dynamic_slice_in_dim(table[layer_index], head_index * head_size, head_size)

        layer_state = state[layer_index, 0].reshape(-1, head_size, head_size)
        out_tile, layer_state = recurrent_update(
            layer_state,
            *output_pieces,
            head_columns(decay_bias_fixed),
            head_columns(self_token_weight),
            head_columns(readout_norm_gain)
        )
        out_all = double_gather(out_tile, position, 0, low_bits, move_outs)
        branch = jnp.dot(out_all, output_weight[layer_index, 0], preferred_element_type=jnp.float32)
        return (branch, layer_state.reshape(layer_state.shape[0], head_size * head_size))

    columns = double_gather(tokens[0], position, low_bits, high_bits, move_rows)
    first_branch, first_memory = mixer(columns, 0)
    summed = double_sum(
        first_branch,
        low_bits,
        high_bits,
        lambda payload, which_bit: swapped(payload, "tp", which_bit),
    )
    columns = (columns.astype(jnp.float32) + summed).astype(jnp.bfloat16)
    second_branch, second_memory = mixer(columns, 1)
    (tile_sum,) = halve_sum((second_branch,), position, low_bits, high_bits, move_split)
    resid_rows = lax.dynamic_slice_in_dim(columns, head_index * seq_tile, seq_tile, 0)
    mixed = (resid_rows.astype(jnp.float32) + tile_sum).astype(jnp.bfloat16)
    new_state = jnp.stack([first_memory, second_memory])[:, None]
    return (mixed[None], new_state)


def solution(mesh):
    return jax.shard_map(
        on_device,
        mesh=mesh,
        in_specs=(
            P("tp", None, None),
            P(),
            P(None, "tp", None, None),
            P(None, "tp", None, None),
            P(None, "tp", None, None),
            P(None, "tp", None, None),
            P(None, "tp", None, None),
            P(None, "tp", None, None),
            P(),
            P(),
            P(),
            P(None, "tp", None, None),
            P(None, "tp", None, None),
        ),
        out_specs=(P("tp", None, None), P(None, "tp", None, None)),
        check_vma=False,
    )
```

profile of v0, /device:TPU:2, one launch (start us, length us, event | category | flops | bytes accessed | tf_op | source)
XLA Modules:
  0.0 315.4 jit_solution(10732244096311176725)
XLA Ops:
  0.6 4.7 %collective-permute-start = (bf16[8,128]{1,0:T(8,128)(2,1)}, bf16[8,128]{1,0:T(8,128)(2,1)S(1)}, u32[]{:S(2)}, u32[]{:S(2)}) collective-permute-start(bf16[8,128]{1,0:T(8,128)(2,1)} %bitcast.109), channel_id=1, source_target_pairs={{0,32},{1,33},{2,34},{3,35},{4,36},{5,37},{6,38},{7,39},{8,40},{9,... | collective-permute-start | bytes 6152 | tf_op jit(solution)/shard_map/ppermute | solution.py:14
  12.3 6.4 %collective-permute-start.1 = (bf16[16,128]{1,0:T(8,128)(2,1)S(1)}, bf16[16,128]{1,0:T(8,128)(2,1)S(1)}, u32[]{:S(2)}, u32[]{:S(2)}) collective-permute-start(bf16[16,128]{1,0:T(8,128)(2,1)S(1)} %maximum_select_fusion.14), channel_id=1, source_target_pairs={{0,64},{1,65},{2,66},{3,67},{4,68},{5,69},{6,70},{7,71},{8,72},{9,... | collective-permute-start | bytes 12296 | tf_op jit(solution)/shard_map/ppermute | solution.py:14
  18.7 3.0 collective-permute-done.1
  21.7 5.2 %collective-permute-start.2 = (bf16[32,128]{1,0:T(8,128)(2,1)S(1)}, bf16[32,128]{1,0:T(8,128)(2,1)S(1)}, u32[]{:S(2)}, u32[]{:S(2)}) collective-permute-start(bf16[32,128]{1,0:T(8,128)(2,1)S(1)} %maximum_select_fusion.11), channel_id=1, source_target_pairs={{0,128},{1,129},{2,130},{3,131},{4,132},{5,133},{6,134},{7,135},{8... | collective-permute-start | bytes 24584 | tf_op jit(solution)/shard_map/ppermute | solution.py:14
  28.5 7.9 %collective-permute-start.3 = (bf16[64,128]{1,0:T(8,128)(2,1)S(1)}, bf16[64,128]{1,0:T(8,128)(2,1)S(1)}, u32[]{:S(2)}, u32[]{:S(2)}) collective-permute-start(bf16[64,128]{1,0:T(8,128)(2,1)S(1)} %maximum_select_fusion.8), channel_id=1, source_target_pairs={{0,256},{1,257},{2,258},{3,259},{4,260},{5,261},{6,262},{7,263},{8... | collective-permute-start | bytes 49160 | tf_op jit(solution)/shard_map/ppermute | solution.py:14
  38.1 11.9 %collective-permute-start.4 = (bf16[128,128]{1,0:T(8,128)(2,1)S(1)}, bf16[128,128]{1,0:T(8,128)(2,1)S(1)}, u32[]{:S(2)}, u32[]{:S(2)}) collective-permute-start(bf16[128,128]{1,0:T(8,128)(2,1)S(1)} %maximum_select_fusion.5), channel_id=1, source_target_pairs={{0,512},{1,513},{2,514},{3,515},{4,516},{5,517},{6,518},{7,519},{8... | collective-permute-start | bytes 98312 | tf_op jit(solution)/shard_map/ppermute | solution.py:14
  52.0 3.6 %collective-permute-start.10 = (f32[128]{0:T(128)S(1)}, f32[128]{0:T(128)S(1)}, u32[]{:S(2)}, u32[]{:S(2)}) collective-permute-start(f32[128]{0:T(128)S(1)} %broadcast_select_fusion.2), channel_id=1, source_target_pairs={{0,16},{1,17},{2,18},{3,19},{4,20},{5,21},{6,22},{7,23},{8,24},{9,... | collective-permute-start | bytes 1544 | tf_op jit(solution)/shard_map/ppermute | solution.py:14
  57.5 6.5 %collective-permute-start.11 = (f32[64]{0:T(128)S(1)}, f32[64]{0:T(128)S(1)}, u32[]{:S(2)}, u32[]{:S(2)}) collective-permute-start(f32[64]{0:T(128)S(1)} %broadcast_select_fusion.6), channel_id=1, source_target_pairs={{0,8},{1,9},{2,10},{3,11},{4,12},{5,13},{6,14},{7,15},{8,0},{9,1},... | collective-permute-start | bytes 776 | tf_op jit(solution)/shard_map/ppermute | solution.py:14
  67.0 4.3 %collective-permute-start.12 = (f32[32]{0:T(128)S(1)}, f32[32]{0:T(128)S(1)}, u32[]{:S(2)}, u32[]{:S(2)}) collective-permute-start(f32[32]{0:T(128)S(1)} %broadcast_select_fusion.10), channel_id=1, source_target_pairs={{0,4},{1,5},{2,6},{3,7},{4,0},{5,1},{6,2},{7,3},{8,12},{9,13},{10,... | collective-permute-start | bytes 392 | tf_op jit(solution)/shard_map/ppermute | solution.py:14
  71.4 3.6 %collective-permute-start.5 = (f32[128,384]{1,0:T(8,128)S(1)}, f32[128,384]{1,0:T(8,128)S(1)}, u32[]{:S(2)}, u32[]{:S(2)}) collective-permute-start(f32[128,384]{1,0:T(8,128)S(1)} %slice_select_fusion.1), channel_id=1, source_target_pairs={{0,16},{1,17},{2,18},{3,19},{4,20},{5,21},{6,22},{7,23},{8,24},{9,... | collective-permute-start | bytes 589832 | tf_op jit(solution)/shard_map/ppermute | solution.py:14
  75.1 3.9 %collective-permute-done.5 = f32[128,384]{1,0:T(8,128)S(1)} collective-permute-done((f32[128,384]{1,0:T(8,128)S(1)}, f32[128,384]{1,0:T(8,128)S(1)}, u32[]{:S(2)}, u32[]{:S(2)}) %collective-permute-start.5) | collective-permute-done | bytes 196640 | tf_op jit(solution)/shard_map/ppermute | solution.py:14
  79.0 4.7 %collective-permute-start.6 = (f32[64,384]{1,0:T(8,128)S(1)}, f32[64,384]{1,0:T(8,128)S(1)}, u32[]{:S(2)}, u32[]{:S(2)}) collective-permute-start(f32[64,384]{1,0:T(8,128)S(1)} %slice_select_fusion.3), channel_id=1, source_target_pairs={{0,8},{1,9},{2,10},{3,11},{4,12},{5,13},{6,14},{7,15},{8,0},{9,1},... | collective-permute-start | bytes 294920 | tf_op jit(solution)/shard_map/ppermute | solution.py:14
  83.8 3.3 %collective-permute-start.13 = (f32[16]{0:T(128)S(1)}, f32[16]{0:T(128)S(1)}, u32[]{:S(2)}, u32[]{:S(2)}) collective-permute-start(f32[16]{0:T(128)S(1)} %broadcast_select_fusion.14), channel_id=1, source_target_pairs={{0,2},{1,3},{2,0},{3,1},{4,6},{5,7},{6,4},{7,5},{8,10},{9,11},{10,... | collective-permute-start | bytes 200 | tf_op jit(solution)/shard_map/ppermute | solution.py:14
  87.1 3.9 %collective-permute-done.6 = f32[64,384]{1,0:T(8,128)S(1)} collective-permute-done((f32[64,384]{1,0:T(8,128)S(1)}, f32[64,384]{1,0:T(8,128)S(1)}, u32[]{:S(2)}, u32[]{:S(2)}) %collective-permute-start.6) | collective-permute-done | bytes 98336 | tf_op jit(solution)/shard_map/ppermute | solution.py:14
  93.1 4.9 %collective-permute-done.7 = f32[32,384]{1,0:T(8,128)S(1)} collective-permute-done((f32[32,384]{1,0:T(8,128)S(1)}, f32[32,384]{1,0:T(8,128)S(1)}, u32[]{:S(2)}, u32[]{:S(2)}) %collective-permute-start.7) | collective-permute-done | bytes 49184 | tf_op jit(solution)/shard_map/ppermute | solution.py:14
  114.2 3.2 %collective-permute-done.16 = bf16[16,64]{1,0:T(8,128)(2,1)S(1)} collective-permute-done((bf16[16,64]{1,0:T(8,128)(2,1)S(1)}, bf16[16,64]{1,0:T(8,128)(2,1)S(1)}, u32[]{:S(2)}, u32[]{:S(2)}) %collective-permute-start.16) | collective-permute-done | bytes 2080 | tf_op jit(solution)/shard_map/ppermute | solution.py:14
  120.1 3.7 %collective-permute-done.17 = bf16[32,64]{1,0:T(8,128)(2,1)S(1)} collective-permute-done((bf16[32,64]{1,0:T(8,128)(2,1)S(1)}, bf16[32,64]{1,0:T(8,128)(2,1)S(1)}, u32[]{:S(2)}, u32[]{:S(2)}) %collective-permute-start.17) | collective-permute-done | bytes 4128 | tf_op jit(solution)/shard_map/ppermute | solution.py:14
  123.8 3.4 %collective-permute-start.18 = (bf16[64,64]{1,0:T(8,128)(2,1)S(1)}, bf16[64,64]{1,0:T(8,128)(2,1)S(1)}, u32[]{:S(2)}, u32[]{:S(2)}) collective-permute-start(bf16[64,64]{1,0:T(8,128)(2,1)S(1)} %maximum_select_fusion.9), channel_id=1, source_target_pairs={{0,8},{1,9},{2,10},{3,11},{4,12},{5,13},{6,14},{7,15},{8,0},{9,1},... | collective-permute-start | bytes 24584 | tf_op jit(solution)/shard_map/ppermute | solution.py:14
  127.3 6.1 %collective-permute-done.18 = bf16[64,64]{1,0:T(8,128)(2,1)S(1)} collective-permute-done((bf16[64,64]{1,0:T(8,128)(2,1)S(1)}, bf16[64,64]{1,0:T(8,128)(2,1)S(1)}, u32[]{:S(2)}, u32[]{:S(2)}) %collective-permute-start.18) | collective-permute-done | bytes 8224 | tf_op jit(solution)/shard_map/ppermute | solution.py:14
  133.4 3.6 %collective-permute-start.19 = (bf16[128,64]{1,0:T(8,128)(2,1)S(1)}, bf16[128,64]{1,0:T(8,128)(2,1)S(1)}, u32[]{:S(2)}, u32[]{:S(2)}) collective-permute-start(bf16[128,64]{1,0:T(8,128)(2,1)S(1)} %maximum_select_fusion.6), channel_id=1, source_target_pairs={{0,16},{1,17},{2,18},{3,19},{4,20},{5,21},{6,22},{7,23},{8,24},{9,... | collective-permute-start | bytes 49160 | tf_op jit(solution)/shard_map/ppermute | solution.py:14
  141.6 5.4 %collective-permute-done.20 = f32[256,128]{1,0:T(8,128)S(1)} collective-permute-done((f32[256,128]{1,0:T(8,128)S(1)}, f32[256,128]{1,0:T(8,128)S(1)}, u32[]{:S(2)}, u32[]{:S(2)}) %collective-permute-start.20) | collective-permute-done | bytes 131104 | tf_op jit(solution)/shard_map/ppermute | solution.py:14
  147.1 9.3 %collective-permute-start.21 = (f32[256,128]{1,0:T(8,128)S(1)}, f32[256,128]{1,0:T(8,128)S(1)}, u32[]{:S(2)}, u32[]{:S(2)}) collective-permute-start(f32[256,128]{1,0:T(8,128)S(1)} %add.249), channel_id=1, source_target_pairs={{0,64},{1,65},{2,66},{3,67},{4,68},{5,69},{6,70},{7,71},{8,72},{9,... | collective-permute-start | bytes 393224 | tf_op jit(solution)/shard_map/ppermute | solution.py:14
  159.4 3.9 %collective-permute-start.22 = (f32[256,128]{1,0:T(8,128)S(1)}, f32[256,128]{1,0:T(8,128)S(1)}, u32[]{:S(2)}, u32[]{:S(2)}) collective-permute-start(f32[256,128]{1,0:T(8,128)S(1)} %add.250), channel_id=1, source_target_pairs={{0,128},{1,129},{2,130},{3,131},{4,132},{5,133},{6,134},{7,135},{8... | collective-permute-start | bytes 393224 | tf_op jit(solution)/shard_map/ppermute | solution.py:14
  163.3 3.9 %collective-permute-done.22 = f32[256,128]{1,0:T(8,128)S(1)} collective-permute-done((f32[256,128]{1,0:T(8,128)S(1)}, f32[256,128]{1,0:T(8,128)S(1)}, u32[]{:S(2)}, u32[]{:S(2)}) %collective-permute-start.22) | collective-permute-done | bytes 131104 | tf_op jit(solution)/shard_map/ppermute | solution.py:14
  167.2 4.5 %collective-permute-start.23 = (f32[256,128]{1,0:T(8,128)S(1)}, f32[256,128]{1,0:T(8,128)S(1)}, u32[]{:S(2)}, u32[]{:S(2)}) collective-permute-start(f32[256,128]{1,0:T(8,128)S(1)} %add.251), channel_id=1, source_target_pairs={{0,256},{1,257},{2,258},{3,259},{4,260},{5,261},{6,262},{7,263},{8... | collective-permute-start | bytes 393224 | tf_op jit(solution)/shard_map/ppermute | solution.py:14
  171.7 3.2 %collective-permute-done.23 = f32[256,128]{1,0:T(8,128)S(1)} collective-permute-done((f32[256,128]{1,0:T(8,128)S(1)}, f32[256,128]{1,0:T(8,128)S(1)}, u32[]{:S(2)}, u32[]{:S(2)}) %collective-permute-start.23) | collective-permute-done | bytes 131104 | tf_op jit(solution)/shard_map/ppermute | solution.py:14
  175.0 11.9 %collective-permute-start.24 = (f32[256,128]{1,0:T(8,128)S(1)}, f32[256,128]{1,0:T(8,128)S(1)}, u32[]{:S(2)}, u32[]{:S(2)}) collective-permute-start(f32[256,128]{1,0:T(8,128)S(1)} %add.252), channel_id=1, source_target_pairs={{0,512},{1,513},{2,514},{3,515},{4,516},{5,517},{6,518},{7,519},{8... | collective-permute-start | bytes 393224 | tf_op jit(solution)/shard_map/ppermute | solution.py:14
  190.0 4.8 %collective-permute-start.30 = (f32[128]{0:T(128)S(1)}, f32[128]{0:T(128)S(1)}, u32[]{:S(2)}, u32[]{:S(2)}) collective-permute-start(f32[128]{0:T(128)S(1)} %broadcast_select_fusion), channel_id=1, source_target_pairs={{0,16},{1,17},{2,18},{3,19},{4,20},{5,21},{6,22},{7,23},{8,24},{9,... | collective-permute-start | bytes 1544 | tf_op jit(solution)/shard_map/ppermute | solution.py:14
  196.4 3.9 %collective-permute-start.31 = (f32[64]{0:T(128)S(1)}, f32[64]{0:T(128)S(1)}, u32[]{:S(2)}, u32[]{:S(2)}) collective-permute-start(f32[64]{0:T(128)S(1)} %broadcast_select_fusion.4), channel_id=1, source_target_pairs={{0,8},{1,9},{2,10},{3,11},{4,12},{5,13},{6,14},{7,15},{8,0},{9,1},... | collective-permute-start | bytes 776 | tf_op jit(solution)/shard_map/ppermute | solution.py:14
  200.5 5.2 %collective-permute-done.31 = f32[64]{0:T(128)S(1)} collective-permute-done((f32[64]{0:T(128)S(1)}, f32[64]{0:T(128)S(1)}, u32[]{:S(2)}, u32[]{:S(2)}) %collective-permute-start.31) | collective-permute-done | bytes 288 | tf_op jit(solution)/shard_map/ppermute | solution.py:14
  207.8 3.9 %collective-permute-start.25 = (f32[128,384]{1,0:T(8,128)S(1)}, f32[128,384]{1,0:T(8,128)S(1)}, u32[]{:S(2)}, u32[]{:S(2)}) collective-permute-start(f32[128,384]{1,0:T(8,128)S(1)} %slice_select_fusion), channel_id=1, source_target_pairs={{0,16},{1,17},{2,18},{3,19},{4,20},{5,21},{6,22},{7,23},{8,24},{9,... | collective-permute-start | bytes 589832 | tf_op jit(solution)/shard_map/ppermute | solution.py:14
  212.3 3.1 collective-permute-done.25
  215.5 6.2 %collective-permute-start.26 = (f32[64,384]{1,0:T(8,128)S(1)}, f32[64,384]{1,0:T(8,128)S(1)}, u32[]{:S(2)}, u32[]{:S(2)}) collective-permute-start(f32[64,384]{1,0:T(8,128)S(1)} %slice_select_fusion.2), channel_id=1, source_target_pairs={{0,8},{1,9},{2,10},{3,11},{4,12},{5,13},{6,14},{7,15},{8,0},{9,1},... | collective-permute-start | bytes 294920 | tf_op jit(solution)/shard_map/ppermute | solution.py:14
  221.8 3.7 %collective-permute-start.33 = (f32[16]{0:T(128)S(1)}, f32[16]{0:T(128)S(1)}, u32[]{:S(2)}, u32[]{:S(2)}) collective-permute-start(f32[16]{0:T(128)S(1)} %broadcast_select_fusion.12), channel_id=1, source_target_pairs={{0,2},{1,3},{2,0},{3,1},{4,6},{5,7},{6,4},{7,5},{8,10},{9,11},{10,... | collective-permute-start | bytes 200 | tf_op jit(solution)/shard_map/ppermute | solution.py:14
  226.0 4.7 %collective-permute-start.27 = (f32[32,384]{1,0:T(8,128)S(1)}, f32[32,384]{1,0:T(8,128)S(1)}, u32[]{:S(2)}, u32[]{:S(2)}) collective-permute-start(f32[32,384]{1,0:T(8,128)S(1)} %slice_select_fusion.4), channel_id=1, source_target_pairs={{0,4},{1,5},{2,6},{3,7},{4,0},{5,1},{6,2},{7,3},{8,12},{9,13},{10,... | collective-permute-start | bytes 147464 | tf_op jit(solution)/shard_map/ppermute | solution.py:14
  232.9 6.0 %collective-permute-start.28 = (f32[16,384]{1,0:T(8,128)S(1)}, f32[16,384]{1,0:T(8,128)S(1)}, u32[]{:S(2)}, u32[]{:S(2)}) collective-permute-start(f32[16,384]{1,0:T(8,128)S(1)} %slice_select_fusion.6), channel_id=1, source_target_pairs={{0,2},{1,3},{2,0},{3,1},{4,6},{5,7},{6,4},{7,5},{8,10},{9,11},{10,... | collective-permute-start | bytes 73736 | tf_op jit(solution)/shard_map/ppermute | solution.py:14
  249.3 3.5 %collective-permute-start.36 = (bf16[16,64]{1,0:T(8,128)(2,1)S(1)}, bf16[16,64]{1,0:T(8,128)(2,1)S(1)}, u32[]{:S(2)}, u32[]{:S(2)}) collective-permute-start(bf16[16,64]{1,0:T(8,128)(2,1)S(1)} %maximum_select_fusion.16), channel_id=1, source_target_pairs={{0,2},{1,3},{2,0},{3,1},{4,6},{5,7},{6,4},{7,5},{8,10},{9,11},{10,... | collective-permute-start | bytes 6152 | tf_op jit(solution)/shard_map/ppermute | solution.py:14
  257.0 4.2 %collective-permute-done.37 = bf16[32,64]{1,0:T(8,128)(2,1)S(1)} collective-permute-done((bf16[32,64]{1,0:T(8,128)(2,1)S(1)}, bf16[32,64]{1,0:T(8,128)(2,1)S(1)}, u32[]{:S(2)}, u32[]{:S(2)}) %collective-permute-start.37) | collective-permute-done | bytes 4128 | tf_op jit(solution)/shard_map/ppermute | solution.py:14
  261.2 5.1 %collective-permute-start.38 = (bf16[64,64]{1,0:T(8,128)(2,1)S(1)}, bf16[64,64]{1,0:T(8,128)(2,1)S(1)}, u32[]{:S(2)}, u32[]{:S(2)}) collective-permute-start(bf16[64,64]{1,0:T(8,128)(2,1)S(1)} %maximum_select_fusion.10), channel_id=1, source_target_pairs={{0,8},{1,9},{2,10},{3,11},{4,12},{5,13},{6,14},{7,15},{8,0},{9,1},... | collective-permute-start | bytes 24584 | tf_op jit(solution)/shard_map/ppermute | solution.py:14
  266.3 4.6 %collective-permute-done.38 = bf16[64,64]{1,0:T(8,128)(2,1)S(1)} collective-permute-done((bf16[64,64]{1,0:T(8,128)(2,1)S(1)}, bf16[64,64]{1,0:T(8,128)(2,1)S(1)}, u32[]{:S(2)}, u32[]{:S(2)}) %collective-permute-start.38) | collective-permute-done | bytes 8224 | tf_op jit(solution)/shard_map/ppermute | solution.py:14
  272.9 3.7 %collective-permute-done.39 = bf16[128,64]{1,0:T(8,128)(2,1)S(1)} collective-permute-done((bf16[128,64]{1,0:T(8,128)(2,1)S(1)}, bf16[128,64]{1,0:T(8,128)(2,1)S(1)}, u32[]{:S(2)}, u32[]{:S(2)}) %collective-permute-start.39) | collective-permute-done | bytes 16416 | tf_op jit(solution)/shard_map/ppermute | solution.py:14
  276.8 5.2 %collective-permute-start.40 = (bf16[128,128]{1,0:T(8,128)(2,1)S(1)}, bf16[128,128]{1,0:T(8,128)(2,1)S(1)}, u32[]{:S(2)}, u32[]{:S(2)}) collective-permute-start(bf16[128,128]{1,0:T(8,128)(2,1)S(1)} %select_convert_fusion), channel_id=1, source_target_pairs={{0,512},{1,513},{2,514},{3,515},{4,516},{5,517},{6,518},{7,519},{8... | collective-permute-start | bytes 98312 | tf_op jit(solution)/shard_map/ppermute | solution.py:14
  282.6 4.3 %collective-permute-done.40 = bf16[128,128]{1,0:T(8,128)(2,1)S(1)} collective-permute-done((bf16[128,128]{1,0:T(8,128)(2,1)S(1)}, bf16[128,128]{1,0:T(8,128)(2,1)S(1)}, u32[]{:S(2)}, u32[]{:S(2)}) %collective-permute-start.40) | collective-permute-done | bytes 32800 | tf_op jit(solution)/shard_map/ppermute | solution.py:14
  289.0 4.5 %collective-permute-done.41 = bf16[64,128]{1,0:T(8,128)(2,1)S(1)} collective-permute-done((bf16[64,128]{1,0:T(8,128)(2,1)S(1)}, bf16[64,128]{1,0:T(8,128)(2,1)S(1)}, u32[]{:S(2)}, u32[]{:S(2)}) %collective-permute-start.41) | collective-permute-done | bytes 16416 | tf_op jit(solution)/shard_map/ppermute | solution.py:14
  295.9 3.1 collective-permute-done.42
  299.0 4.6 %collective-permute-start.43 = (bf16[16,128]{1,0:T(8,128)(2,1)S(1)}, bf16[16,128]{1,0:T(8,128)(2,1)S(1)}, u32[]{:S(2)}, u32[]{:S(2)}) collective-permute-start(bf16[16,128]{1,0:T(8,128)(2,1)S(1)} %select_convert_fusion.3), channel_id=1, source_target_pairs={{0,64},{1,65},{2,66},{3,67},{4,68},{5,69},{6,70},{7,71},{8,72},{9,... | collective-permute-start | bytes 12296 | tf_op jit(solution)/shard_map/ppermute | solution.py:14
  303.7 4.8 %collective-permute-done.43 = bf16[16,128]{1,0:T(8,128)(2,1)S(1)} collective-permute-done((bf16[16,128]{1,0:T(8,128)(2,1)S(1)}, bf16[16,128]{1,0:T(8,128)(2,1)S(1)}, u32[]{:S(2)}, u32[]{:S(2)}) %collective-permute-start.43) | collective-permute-done | bytes 4128 | tf_op jit(solution)/shard_map/ppermute | solution.py:14
  311.1 3.7 %collective-permute-done.44 = bf16[8,128]{1,0:T(8,128)(2,1)S(1)} collective-permute-done((bf16[8,128]{1,0:T(8,128)(2,1)S(1)}, bf16[8,128]{1,0:T(8,128)(2,1)S(1)}, u32[]{:S(2)}, u32[]{:S(2)}) %collective-permute-start.44) | collective-permute-done | bytes 2080 | tf_op jit(solution)/shard_map/ppermute | solution.py:14
  (191 shorter events, 81.0 us)
Async XLA Ops:
  0.6 11.0 %collective-permute-start = (bf16[8,128]{1,0:T(8,128)(2,1)}, bf16[8,128]{1,0:T(8,128)(2,1)S(1)}, u32[]{:S(2)}, u32[]{:S(2)}) collective-permute-start(bf16[8,128]{1,0:T(8,128)(2,1)} %bitcast.109), channel_id=1, source_target_pairs={{0,32},{1,33},{2,34},{3,35},{4,36},{5,37},{6,38},{7,39},{8,40},{9,... | collective-permute-start | bytes 6152 | tf_op jit(solution)/shard_map/ppermute | solution.py:14
  11.6 7.1 %copy-start.6 = (bf16[2,1,128,64]{2,3,1,0:T(8,128)(2,1)S(1)}, bf16[2,1,128,64]{2,3,1,0:T(8,128)(2,1)}, u32[]{:S(2)}) copy-start(bf16[2,1,128,64]{2,3,1,0:T(8,128)(2,1)} %param.20) | copy-start | bytes 98308
  12.3 9.4 %collective-permute-start.1 = (bf16[16,128]{1,0:T(8,128)(2,1)S(1)}, bf16[16,128]{1,0:T(8,128)(2,1)S(1)}, u32[]{:S(2)}, u32[]{:S(2)}) collective-permute-start(bf16[16,128]{1,0:T(8,128)(2,1)S(1)} %maximum_select_fusion.14), channel_id=1, source_target_pairs={{0,64},{1,65},{2,66},{3,67},{4,68},{5,69},{6,70},{7,71},{8,72},{9,... | collective-permute-start | bytes 12296 | tf_op jit(solution)/shard_map/ppermute | solution.py:14
  21.7 6.8 %collective-permute-start.2 = (bf16[32,128]{1,0:T(8,128)(2,1)S(1)}, bf16[32,128]{1,0:T(8,128)(2,1)S(1)}, u32[]{:S(2)}, u32[]{:S(2)}) collective-permute-start(bf16[32,128]{1,0:T(8,128)(2,1)S(1)} %maximum_select_fusion.11), channel_id=1, source_target_pairs={{0,128},{1,129},{2,130},{3,131},{4,132},{5,133},{6,134},{7,135},{8... | collective-permute-start | bytes 24584 | tf_op jit(solution)/shard_map/ppermute | solution.py:14
  28.5 9.6 %collective-permute-start.3 = (bf16[64,128]{1,0:T(8,128)(2,1)S(1)}, bf16[64,128]{1,0:T(8,128)(2,1)S(1)}, u32[]{:S(2)}, u32[]{:S(2)}) collective-permute-start(bf16[64,128]{1,0:T(8,128)(2,1)S(1)} %maximum_select_fusion.8), channel_id=1, source_target_pairs={{0,256},{1,257},{2,258},{3,259},{4,260},{5,261},{6,262},{7,263},{8... | collective-permute-start | bytes 49160 | tf_op jit(solution)/shard_map/ppermute | solution.py:14
  38.1 13.7 %collective-permute-start.4 = (bf16[128,128]{1,0:T(8,128)(2,1)S(1)}, bf16[128,128]{1,0:T(8,128)(2,1)S(1)}, u32[]{:S(2)}, u32[]{:S(2)}) collective-permute-start(bf16[128,128]{1,0:T(8,128)(2,1)S(1)} %maximum_select_fusion.5), channel_id=1, source_target_pairs={{0,512},{1,513},{2,514},{3,515},{4,516},{5,517},{6,518},{7,519},{8... | collective-permute-start | bytes 98312 | tf_op jit(solution)/shard_map/ppermute | solution.py:14
  52.0 5.5 %collective-permute-start.10 = (f32[128]{0:T(128)S(1)}, f32[128]{0:T(128)S(1)}, u32[]{:S(2)}, u32[]{:S(2)}) collective-permute-start(f32[128]{0:T(128)S(1)} %broadcast_select_fusion.2), channel_id=1, source_target_pairs={{0,16},{1,17},{2,18},{3,19},{4,20},{5,21},{6,22},{7,23},{8,24},{9,... | collective-permute-start | bytes 1544 | tf_op jit(solution)/shard_map/ppermute | solution.py:14
  57.5 9.4 %collective-permute-start.11 = (f32[64]{0:T(128)S(1)}, f32[64]{0:T(128)S(1)}, u32[]{:S(2)}, u32[]{:S(2)}) collective-permute-start(f32[64]{0:T(128)S(1)} %broadcast_select_fusion.6), channel_id=1, source_target_pairs={{0,8},{1,9},{2,10},{3,11},{4,12},{5,13},{6,14},{7,15},{8,0},{9,1},... | collective-permute-start | bytes 776 | tf_op jit(solution)/shard_map/ppermute | solution.py:14
  67.0 8.0 %collective-permute-start.12 = (f32[32]{0:T(128)S(1)}, f32[32]{0:T(128)S(1)}, u32[]{:S(2)}, u32[]{:S(2)}) collective-permute-start(f32[32]{0:T(128)S(1)} %broadcast_select_fusion.10), channel_id=1, source_target_pairs={{0,4},{1,5},{2,6},{3,7},{4,0},{5,1},{6,2},{7,3},{8,12},{9,13},{10,... | collective-permute-start | bytes 392 | tf_op jit(solution)/shard_map/ppermute | solution.py:14
  71.4 7.6 %collective-permute-start.5 = (f32[128,384]{1,0:T(8,128)S(1)}, f32[128,384]{1,0:T(8,128)S(1)}, u32[]{:S(2)}, u32[]{:S(2)}) collective-permute-start(f32[128,384]{1,0:T(8,128)S(1)} %slice_select_fusion.1), channel_id=1, source_target_pairs={{0,16},{1,17},{2,18},{3,19},{4,20},{5,21},{6,22},{7,23},{8,24},{9,... | collective-permute-start | bytes 589832 | tf_op jit(solution)/shard_map/ppermute | solution.py:14
  79.0 12.0 %collective-permute-start.6 = (f32[64,384]{1,0:T(8,128)S(1)}, f32[64,384]{1,0:T(8,128)S(1)}, u32[]{:S(2)}, u32[]{:S(2)}) collective-permute-start(f32[64,384]{1,0:T(8,128)S(1)} %slice_select_fusion.3), channel_id=1, source_target_pairs={{0,8},{1,9},{2,10},{3,11},{4,12},{5,13},{6,14},{7,15},{8,0},{9,1},... | collective-permute-start | bytes 294920 | tf_op jit(solution)/shard_map/ppermute | solution.py:14
  83.8 9.2 %collective-permute-start.13 = (f32[16]{0:T(128)S(1)}, f32[16]{0:T(128)S(1)}, u32[]{:S(2)}, u32[]{:S(2)}) collective-permute-start(f32[16]{0:T(128)S(1)} %broadcast_select_fusion.14), channel_id=1, source_target_pairs={{0,2},{1,3},{2,0},{3,1},{4,6},{5,7},{6,4},{7,5},{8,10},{9,11},{10,... | collective-permute-start | bytes 200 | tf_op jit(solution)/shard_map/ppermute | solution.py:14
  91.1 6.9 %collective-permute-start.7 = (f32[32,384]{1,0:T(8,128)S(1)}, f32[32,384]{1,0:T(8,128)S(1)}, u32[]{:S(2)}, u32[]{:S(2)}) collective-permute-start(f32[32,384]{1,0:T(8,128)S(1)} %slice_select_fusion.5), channel_id=1, source_target_pairs={{0,4},{1,5},{2,6},{3,7},{4,0},{5,1},{6,2},{7,3},{8,12},{9,13},{10,... | collective-permute-start | bytes 147464 | tf_op jit(solution)/shard_map/ppermute | solution.py:14
  98.0 5.7 %collective-permute-start.8 = (f32[16,384]{1,0:T(8,128)S(1)}, f32[16,384]{1,0:T(8,128)S(1)}, u32[]{:S(2)}, u32[]{:S(2)}) collective-permute-start(f32[16,384]{1,0:T(8,128)S(1)} %slice_select_fusion.7), channel_id=1, source_target_pairs={{0,2},{1,3},{2,0},{3,1},{4,6},{5,7},{6,4},{7,5},{8,10},{9,11},{10,... | collective-permute-start | bytes 73736 | tf_op jit(solution)/shard_map/ppermute | solution.py:14
  100.0 5.7 %collective-permute-start.14 = (f32[8]{0:T(128)S(1)}, f32[8]{0:T(128)S(1)}, u32[]{:S(2)}, u32[]{:S(2)}) collective-permute-start(f32[8]{0:T(128)S(1)} %broadcast_select_fusion.18), channel_id=1, source_target_pairs={{0,1},{1,0},{2,3},{3,2},{4,5},{5,4},{6,7},{7,6},{8,9},{9,8},{10,11... | collective-permute-start | bytes 104 | tf_op jit(solution)/shard_map/ppermute | solution.py:14
  103.7 3.1 collective-permute-start.9
  108.8 3.1 collective-permute-start.15
  111.9 5.5 %collective-permute-start.16 = (bf16[16,64]{1,0:T(8,128)(2,1)S(1)}, bf16[16,64]{1,0:T(8,128)(2,1)S(1)}, u32[]{:S(2)}, u32[]{:S(2)}) collective-permute-start(bf16[16,64]{1,0:T(8,128)(2,1)S(1)} %maximum_select_fusion.15), channel_id=1, source_target_pairs={{0,2},{1,3},{2,0},{3,1},{4,6},{5,7},{6,4},{7,5},{8,10},{9,11},{10,... | collective-permute-start | bytes 6152 | tf_op jit(solution)/shard_map/ppermute | solution.py:14
  117.4 6.4 %collective-permute-start.17 = (bf16[32,64]{1,0:T(8,128)(2,1)S(1)}, bf16[32,64]{1,0:T(8,128)(2,1)S(1)}, u32[]{:S(2)}, u32[]{:S(2)}) collective-permute-start(bf16[32,64]{1,0:T(8,128)(2,1)S(1)} %maximum_select_fusion.12), channel_id=1, source_target_pairs={{0,4},{1,5},{2,6},{3,7},{4,0},{5,1},{6,2},{7,3},{8,12},{9,13},{10,... | collective-permute-start | bytes 12296 | tf_op jit(solution)/shard_map/ppermute | solution.py:14
  123.8 9.5 %collective-permute-start.18 = (bf16[64,64]{1,0:T(8,128)(2,1)S(1)}, bf16[64,64]{1,0:T(8,128)(2,1)S(1)}, u32[]{:S(2)}, u32[]{:S(2)}) collective-permute-start(bf16[64,64]{1,0:T(8,128)(2,1)S(1)} %maximum_select_fusion.9), channel_id=1, source_target_pairs={{0,8},{1,9},{2,10},{3,11},{4,12},{5,13},{6,14},{7,15},{8,0},{9,1},... | collective-permute-start | bytes 24584 | tf_op jit(solution)/shard_map/ppermute | solution.py:14
  127.2 11.9 %copy-start.11 = (bf16[2,1,64,128]{3,2,1,0:T(8,128)(2,1)S(1)}, bf16[2,1,64,128]{3,2,1,0:T(8,128)(2,1)}, u32[]{:S(2)}) copy-start(bf16[2,1,64,128]{3,2,1,0:T(8,128)(2,1)} %param.24) | copy-start | bytes 98308
  133.4 5.8 %collective-permute-start.19 = (bf16[128,64]{1,0:T(8,128)(2,1)S(1)}, bf16[128,64]{1,0:T(8,128)(2,1)S(1)}, u32[]{:S(2)}, u32[]{:S(2)}) collective-permute-start(bf16[128,64]{1,0:T(8,128)(2,1)S(1)} %maximum_select_fusion.6), channel_id=1, source_target_pairs={{0,16},{1,17},{2,18},{3,19},{4,20},{5,21},{6,22},{7,23},{8,24},{9,... | collective-permute-start | bytes 49160 | tf_op jit(solution)/shard_map/ppermute | solution.py:14
  139.3 7.8 %collective-permute-start.20 = (f32[256,128]{1,0:T(8,128)S(1)}, f32[256,128]{1,0:T(8,128)S(1)}, u32[]{:S(2)}, u32[]{:S(2)}) collective-permute-start(f32[256,128]{1,0:T(8,128)S(1)} %fusion.23), channel_id=1, source_target_pairs={{0,32},{1,33},{2,34},{3,35},{4,36},{5,37},{6,38},{7,39},{8,40},{9,... | collective-permute-start | bytes 393224 | tf_op jit(solution)/shard_map/ppermute | solution.py:14
  147.1 12.3 %collective-permute-start.21 = (f32[256,128]{1,0:T(8,128)S(1)}, f32[256,128]{1,0:T(8,128)S(1)}, u32[]{:S(2)}, u32[]{:S(2)}) collective-permute-start(f32[256,128]{1,0:T(8,128)S(1)} %add.249), channel_id=1, source_target_pairs={{0,64},{1,65},{2,66},{3,67},{4,68},{5,69},{6,70},{7,71},{8,72},{9,... | collective-permute-start | bytes 393224 | tf_op jit(solution)/shard_map/ppermute | solution.py:14
  159.4 7.8 %collective-permute-start.22 = (f32[256,128]{1,0:T(8,128)S(1)}, f32[256,128]{1,0:T(8,128)S(1)}, u32[]{:S(2)}, u32[]{:S(2)}) collective-permute-start(f32[256,128]{1,0:T(8,128)S(1)} %add.250), channel_id=1, source_target_pairs={{0,128},{1,129},{2,130},{3,131},{4,132},{5,133},{6,134},{7,135},{8... | collective-permute-start | bytes 393224 | tf_op jit(solution)/shard_map/ppermute | solution.py:14
  167.2 7.8 %collective-permute-start.23 = (f32[256,128]{1,0:T(8,128)S(1)}, f32[256,128]{1,0:T(8,128)S(1)}, u32[]{:S(2)}, u32[]{:S(2)}) collective-permute-start(f32[256,128]{1,0:T(8,128)S(1)} %add.251), channel_id=1, source_target_pairs={{0,256},{1,257},{2,258},{3,259},{4,260},{5,261},{6,262},{7,263},{8... | collective-permute-start | bytes 393224 | tf_op jit(solution)/shard_map/ppermute | solution.py:14
  175.0 14.9 %collective-permute-start.24 = (f32[256,128]{1,0:T(8,128)S(1)}, f32[256,128]{1,0:T(8,128)S(1)}, u32[]{:S(2)}, u32[]{:S(2)}) collective-permute-start(f32[256,128]{1,0:T(8,128)S(1)} %add.252), channel_id=1, source_target_pairs={{0,512},{1,513},{2,514},{3,515},{4,516},{5,517},{6,518},{7,519},{8... | collective-permute-start | bytes 393224 | tf_op jit(solution)/shard_map/ppermute | solution.py:14
  190.0 6.3 %collective-permute-start.30 = (f32[128]{0:T(128)S(1)}, f32[128]{0:T(128)S(1)}, u32[]{:S(2)}, u32[]{:S(2)}) collective-permute-start(f32[128]{0:T(128)S(1)} %broadcast_select_fusion), channel_id=1, source_target_pairs={{0,16},{1,17},{2,18},{3,19},{4,20},{5,21},{6,22},{7,23},{8,24},{9,... | collective-permute-start | bytes 1544 | tf_op jit(solution)/shard_map/ppermute | solution.py:14
  196.4 9.4 %collective-permute-start.31 = (f32[64]{0:T(128)S(1)}, f32[64]{0:T(128)S(1)}, u32[]{:S(2)}, u32[]{:S(2)}) collective-permute-start(f32[64]{0:T(128)S(1)} %broadcast_select_fusion.4), channel_id=1, source_target_pairs={{0,8},{1,9},{2,10},{3,11},{4,12},{5,13},{6,14},{7,15},{8,0},{9,1},... | collective-permute-start | bytes 776 | tf_op jit(solution)/shard_map/ppermute | solution.py:14
  205.9 6.3 %collective-permute-start.32 = (f32[32]{0:T(128)S(1)}, f32[32]{0:T(128)S(1)}, u32[]{:S(2)}, u32[]{:S(2)}) collective-permute-start(f32[32]{0:T(128)S(1)} %broadcast_select_fusion.8), channel_id=1, source_target_pairs={{0,4},{1,5},{2,6},{3,7},{4,0},{5,1},{6,2},{7,3},{8,12},{9,13},{10,... | collective-permute-start | bytes 392 | tf_op jit(solution)/shard_map/ppermute | solution.py:14
  207.8 7.6 %collective-permute-start.25 = (f32[128,384]{1,0:T(8,128)S(1)}, f32[128,384]{1,0:T(8,128)S(1)}, u32[]{:S(2)}, u32[]{:S(2)}) collective-permute-start(f32[128,384]{1,0:T(8,128)S(1)} %slice_select_fusion), channel_id=1, source_target_pairs={{0,16},{1,17},{2,18},{3,19},{4,20},{5,21},{6,22},{7,23},{8,24},{9,... | collective-permute-start | bytes 589832 | tf_op jit(solution)/shard_map/ppermute | solution.py:14
  215.5 10.5 %collective-permute-start.26 = (f32[64,384]{1,0:T(8,128)S(1)}, f32[64,384]{1,0:T(8,128)S(1)}, u32[]{:S(2)}, u32[]{:S(2)}) collective-permute-start(f32[64,384]{1,0:T(8,128)S(1)} %slice_select_fusion.2), channel_id=1, source_target_pairs={{0,8},{1,9},{2,10},{3,11},{4,12},{5,13},{6,14},{7,15},{8,0},{9,1},... | collective-permute-start | bytes 294920 | tf_op jit(solution)/shard_map/ppermute | solution.py:14
  221.8 9.0 %collective-permute-start.33 = (f32[16]{0:T(128)S(1)}, f32[16]{0:T(128)S(1)}, u32[]{:S(2)}, u32[]{:S(2)}) collective-permute-start(f32[16]{0:T(128)S(1)} %broadcast_select_fusion.12), channel_id=1, source_target_pairs={{0,2},{1,3},{2,0},{3,1},{4,6},{5,7},{6,4},{7,5},{8,10},{9,11},{10,... | collective-permute-start | bytes 200 | tf_op jit(solution)/shard_map/ppermute | solution.py:14
  226.0 6.9 %collective-permute-start.27 = (f32[32,384]{1,0:T(8,128)S(1)}, f32[32,384]{1,0:T(8,128)S(1)}, u32[]{:S(2)}, u32[]{:S(2)}) collective-permute-start(f32[32,384]{1,0:T(8,128)S(1)} %slice_select_fusion.4), channel_id=1, source_target_pairs={{0,4},{1,5},{2,6},{3,7},{4,0},{5,1},{6,2},{7,3},{8,12},{9,13},{10,... | collective-permute-start | bytes 147464 | tf_op jit(solution)/shard_map/ppermute | solution.py:14
  232.9 8.0 %collective-permute-start.28 = (f32[16,384]{1,0:T(8,128)S(1)}, f32[16,384]{1,0:T(8,128)S(1)}, u32[]{:S(2)}, u32[]{:S(2)}) collective-permute-start(f32[16,384]{1,0:T(8,128)S(1)} %slice_select_fusion.6), channel_id=1, source_target_pairs={{0,2},{1,3},{2,0},{3,1},{4,6},{5,7},{6,4},{7,5},{8,10},{9,11},{10,... | collective-permute-start | bytes 73736 | tf_op jit(solution)/shard_map/ppermute | solution.py:14
  239.0 4.4 %collective-permute-start.34 = (f32[8]{0:T(128)S(1)}, f32[8]{0:T(128)S(1)}, u32[]{:S(2)}, u32[]{:S(2)}) collective-permute-start(f32[8]{0:T(128)S(1)} %broadcast_select_fusion.16), channel_id=1, source_target_pairs={{0,1},{1,0},{2,3},{3,2},{4,5},{5,4},{6,7},{7,6},{8,9},{9,8},{10,11... | collective-permute-start | bytes 104 | tf_op jit(solution)/shard_map/ppermute | solution.py:14
  241.0 3.2 %collective-permute-start.29 = (f32[8,384]{1,0:T(8,128)S(1)}, f32[8,384]{1,0:T(8,128)S(1)}, u32[]{:S(2)}, u32[]{:S(2)}) collective-permute-start(f32[8,384]{1,0:T(8,128)S(1)} %slice_select_fusion.8), channel_id=1, source_target_pairs={{0,1},{1,0},{2,3},{3,2},{4,5},{5,4},{6,7},{7,6},{8,9},{9,8},{10,11... | collective-permute-start | bytes 36872 | tf_op jit(solution)/shard_map/ppermute | solution.py:14
  246.2 3.1 collective-permute-start.35
  249.3 5.5 %collective-permute-start.36 = (bf16[16,64]{1,0:T(8,128)(2,1)S(1)}, bf16[16,64]{1,0:T(8,128)(2,1)S(1)}, u32[]{:S(2)}, u32[]{:S(2)}) collective-permute-start(bf16[16,64]{1,0:T(8,128)(2,1)S(1)} %maximum_select_fusion.16), channel_id=1, source_target_pairs={{0,2},{1,3},{2,0},{3,1},{4,6},{5,7},{6,4},{7,5},{8,10},{9,11},{10,... | collective-permute-start | bytes 6152 | tf_op jit(solution)/shard_map/ppermute | solution.py:14
  254.8 6.4 %collective-permute-start.37 = (bf16[32,64]{1,0:T(8,128)(2,1)S(1)}, bf16[32,64]{1,0:T(8,128)(2,1)S(1)}, u32[]{:S(2)}, u32[]{:S(2)}) collective-permute-start(bf16[32,64]{1,0:T(8,128)(2,1)S(1)} %maximum_select_fusion.13), channel_id=1, source_target_pairs={{0,4},{1,5},{2,6},{3,7},{4,0},{5,1},{6,2},{7,3},{8,12},{9,13},{10,... | collective-permute-start | bytes 12296 | tf_op jit(solution)/shard_map/ppermute | solution.py:14
  261.2 9.6 %collective-permute-start.38 = (bf16[64,64]{1,0:T(8,128)(2,1)S(1)}, bf16[64,64]{1,0:T(8,128)(2,1)S(1)}, u32[]{:S(2)}, u32[]{:S(2)}) collective-permute-start(bf16[64,64]{1,0:T(8,128)(2,1)S(1)} %maximum_select_fusion.10), channel_id=1, source_target_pairs={{0,8},{1,9},{2,10},{3,11},{4,12},{5,13},{6,14},{7,15},{8,0},{9,1},... | collective-permute-start | bytes 24584 | tf_op jit(solution)/shard_map/ppermute | solution.py:14
  270.9 5.8 %collective-permute-start.39 = (bf16[128,64]{1,0:T(8,128)(2,1)S(1)}, bf16[128,64]{1,0:T(8,128)(2,1)S(1)}, u32[]{:S(2)}, u32[]{:S(2)}) collective-permute-start(bf16[128,64]{1,0:T(8,128)(2,1)S(1)} %maximum_select_fusion.7), channel_id=1, source_target_pairs={{0,16},{1,17},{2,18},{3,19},{4,20},{5,21},{6,22},{7,23},{8,24},{9,... | collective-permute-start | bytes 49160 | tf_op jit(solution)/shard_map/ppermute | solution.py:14
  276.8 10.1 %collective-permute-start.40 = (bf16[128,128]{1,0:T(8,128)(2,1)S(1)}, bf16[128,128]{1,0:T(8,128)(2,1)S(1)}, u32[]{:S(2)}, u32[]{:S(2)}) collective-permute-start(bf16[128,128]{1,0:T(8,128)(2,1)S(1)} %select_convert_fusion), channel_id=1, source_target_pairs={{0,512},{1,513},{2,514},{3,515},{4,516},{5,517},{6,518},{7,519},{8... | collective-permute-start | bytes 98312 | tf_op jit(solution)/shard_map/ppermute | solution.py:14
  286.9 6.5 %collective-permute-start.41 = (bf16[64,128]{1,0:T(8,128)(2,1)S(1)}, bf16[64,128]{1,0:T(8,128)(2,1)S(1)}, u32[]{:S(2)}, u32[]{:S(2)}) collective-permute-start(bf16[64,128]{1,0:T(8,128)(2,1)S(1)} %select_convert_fusion.1), channel_id=1, source_target_pairs={{0,256},{1,257},{2,258},{3,259},{4,260},{5,261},{6,262},{7,263},{8... | collective-permute-start | bytes 49160 | tf_op jit(solution)/shard_map/ppermute | solution.py:14
  293.5 5.5 %collective-permute-start.42 = (bf16[32,128]{1,0:T(8,128)(2,1)S(1)}, bf16[32,128]{1,0:T(8,128)(2,1)S(1)}, u32[]{:S(2)}, u32[]{:S(2)}) collective-permute-start(bf16[32,128]{1,0:T(8,128)(2,1)S(1)} %select_convert_fusion.2), channel_id=1, source_target_pairs={{0,128},{1,129},{2,130},{3,131},{4,132},{5,133},{6,134},{7,135},{8... | collective-permute-start | bytes 24584 | tf_op jit(solution)/shard_map/ppermute | solution.py:14
  295.8 7.8 %copy-start = (f32[2,1,8,4096]{3,2,1,0:T(8,128)S(1)}, f32[2,1,8,4096]{3,2,1,0:T(8,128)}, u32[]{:S(2)}) copy-start(f32[2,1,8,4096]{3,2,1,0:T(8,128)} %param.25) | copy-start | bytes 786436
  299.0 9.4 %collective-permute-start.43 = (bf16[16,128]{1,0:T(8,128)(2,1)S(1)}, bf16[16,128]{1,0:T(8,128)(2,1)S(1)}, u32[]{:S(2)}, u32[]{:S(2)}) collective-permute-start(bf16[16,128]{1,0:T(8,128)(2,1)S(1)} %select_convert_fusion.3), channel_id=1, source_target_pairs={{0,64},{1,65},{2,66},{3,67},{4,68},{5,69},{6,70},{7,71},{8,72},{9,... | collective-permute-start | bytes 12296 | tf_op jit(solution)/shard_map/ppermute | solution.py:14
  308.5 6.4 %collective-permute-start.44 = (bf16[8,128]{1,0:T(8,128)(2,1)S(1)}, bf16[8,128]{1,0:T(8,128)(2,1)S(1)}, u32[]{:S(2)}, u32[]{:S(2)}) collective-permute-start(bf16[8,128]{1,0:T(8,128)(2,1)S(1)} %select_convert_fusion.4), channel_id=1, source_target_pairs={{0,32},{1,33},{2,34},{3,35},{4,36},{5,37},{6,38},{7,39},{8,40},{9,... | collective-permute-start | bytes 6152 | tf_op jit(solution)/shard_map/ppermute | solution.py:14
  (9 other events, 11.6 us)
where the time goes:
time: 317 us; the launch traced here: 315 us
  starting transfers between devices  186 us (59%)
  waiting for transfers between devices  111 us (35%)
  local copies, waits for them, and re-layouts  8.13 us (3%)
  other arithmetic  5.29 us (2%)
    ppermute x45, starting transfers between devices, swapped(): lax.ppermute(shard, axis, [(i, i ^ 1 << stride) for i in range(lax.axis_s...  186 us
    ppermute x45, waiting for transfers between devices, swapped(): lax.ppermute(shard, axis, [(i, i ^ 1 << stride) for i in range(lax.axis_s...  111 us
  transfers between devices with their start and end apart: 45, of which 38 were waited for; matrix products, arithmetic and copies ran while one was open for 2% of the time, Pallas kernels for 0%

commit v1 on v0

v1 whole, which is shorter than its diff:
```python
import functools
import math

import jax
import jax.numpy as jnp
from jax import lax
from jax.experimental import pallas as pl
from jax.experimental.pallas import tpu as pltpu
from jax.sharding import PartitionSpec as P

D = 4096
RMS_EPS = 1e-06
GROUP_EPS = 0.00064
MESH = pl.DeviceIdType.MESH
F32 = jnp.float32
BF16 = jnp.bfloat16


def both_halves(tile, low):
    turned = pltpu.roll(tile, 64, 1)
    return jnp.where(low, tile, turned), jnp.where(low, turned, tile)


def half_sums(values, ones):
    flat = values.reshape(256, 128)
    high = flat.astype(BF16)
    rest = (flat - high.astype(F32)).astype(BF16)
    total = jnp.dot(high, ones, preferred_element_type=F32)
    total = total + jnp.dot(rest, ones, preferred_element_type=F32)
    return total.reshape(32, 8, 128)


def kernel(
    tokens,
    gain,
    w0,
    w1,
    w2,
    w3,
    w4,
    w5,
    bias,
    selfw,
    rgain,
    wout,
    state,
    mixed,
    new_state,
    xt,
    xbuf,
    wraw,
    wq,
    pbuf,
    rbuf,
    osend,
    obuf,
    wo,
    st,
    sn,
    vgain,
    vbias,
    vself,
    vrgain,
    lsem,
    ssem,
    rsem,
):
    me = lax.axis_index("tp")
    h = lax.div(me, 32)
    b = lax.rem(me, 32)
    core = lax.rem(me, 2)
    x = lax.rem(lax.div(me, 2), 8)
    ylo = lax.rem(lax.div(me, 16), 2)
    z2 = lax.div(h, 16)
    hx = lax.rem(lax.div(h, 2), 8)
    h0 = lax.rem(h, 2)
    jq = ylo * 2 + core

    loads = []

    def load(src, dst, sem):
        copy = pltpu.make_async_copy(src, dst, sem)
        copy.start()
        loads.append(copy)
        return copy

    tok_load = load(tokens.at[0], xt.at[0], lsem.at[0])
    w_loads = []
    for layer in range(2):
        for i, w in enumerate((w0, w1, w2, w3, w4, w5)):
            w_loads.append(load(w.at[layer, 0], wraw.at[layer, i], lsem.at[1 + layer * 6 + i]))
    wo_loads = [load(wout.at[l, 0], wo.at[l, h], lsem.at[13 + l]) for l in range(2)]
    gain_load = load(gain, vgain, lsem.at[15])
    bias_load = load(bias, vbias, lsem.at[16])
    self_load = load(selfw, vself, lsem.at[17])
    rgain_load = load(rgain, vrgain, lsem.at[18])
    st_loads = [load(state.at[l, 0], st.at[l], lsem.at[19 + l]) for l in range(2)]

    def tile_dest(i):
        other = lax.rem(h + 16 + i, 32)
        return other * 32 + z2 * 16 + x * 2 + h0

    def tile_source(i):
        return (ylo * 16 + lax.div(i, 4) * 2 + core) * 32 + lax.div(lax.rem(i, 4), 2) * 16 + x * 2 + lax.rem(i, 2)

    def x_partner(d):
        return me - x * 2 + lax.rem(x + d, 8) * 2

    def quad_partner(d):
        other = lax.rem(jq + d, 4)
        return me - ylo * 16 - core + lax.div(other, 2) * 16 + lax.rem(other, 2)

    def owner_dest(i):
        return b * 32 + lax.rem(lax.rem(me, 32) + 16 + i, 32)

    def head_partner(i):
        return lax.rem(h + i, 32) * 32 + b

    tile_self = jnp.logical_and(z2 == ylo, h0 == core)
    owner_self = h == b

    barrier = pltpu.get_barrier_semaphore()

    def greet(device):
        pl.semaphore_signal(barrier, inc=1, device_id=(device,), device_id_type=MESH)

    def greet_source(i, carry):
        @pl.when(tile_source(i) != me)
        def _():
            greet(tile_source(i))

        return carry

    lax.fori_loop(0, 32, greet_source, 0)
    for d in range(1, 8):
        greet(x_partner(d))
    for d in range(1, 4):
        greet(quad_partner(d))

    def own_weights(layer):
        for i in range(3):
            w_loads[layer * 6 + 2 * i].wait()
            w_loads[layer * 6 + 2 * i + 1].wait()
            pair = jnp.concatenate([wraw[layer, 2 * i], wraw[layer, 2 * i + 1]], axis=1)
            wq[layer, jq, :, 128 * i : 128 * i + 128] = pair

    own_weights(0)
    own_weights(1)
    tok_load.wait()

    @pl.when(tile_self)
    def _():
        pl.semaphore_wait(barrier, 41)

    @pl.when(jnp.logical_not(tile_self))
    def _():
        pl.semaphore_wait(barrier, 42)

    lane = lax.broadcasted_iota(jnp.int32, (8, 128), 1)
    low = lane < 64
    tile3 = lax.broadcasted_iota(jnp.int32, (32, 8, 128), 0)
    lane3 = lax.broadcasted_iota(jnp.int32, (32, 8, 128), 2)
    pick = jnp.logical_or(lane3 == 2 * tile3, lane3 == 2 * tile3 + 65)
    row_half = lax.broadcasted_iota(jnp.int32, (128, 128), 0) < 64
    col_half = lax.broadcasted_iota(jnp.int32, (128, 128), 1) < 64
    ones = jnp.where(row_half == col_half, 1.0, 0.0).astype(BF16)

    def remote(src, dst, phase, layer, device):
        return pltpu.make_async_remote_copy(
            src_ref=src,
            dst_ref=dst,
            send_sem=ssem.at[layer, phase],
            recv_sem=rsem.at[layer, phase],
            device_id=(device,),
            device_id_type=MESH,
        )

    def send_tiles(layer):
        slot = hx * 4 + jq

        def body(i, carry):
            dest = tile_dest(i)

            @pl.when(dest != me)
            def _():
                remote(xt.at[layer], xbuf.at[layer, slot], 0, layer, dest).start()

            return carry

        lax.fori_loop(0, 32, body, 0)

        @pl.when(tile_self)
        def _():
            xbuf[layer, slot] = xt[layer]

    def wait_bytes(ref, sem):
        pltpu.make_async_copy(ref, ref, sem).wait()

    def wait_counted(buf, layer, sem, fewer):
        @pl.when(fewer)
        def _():
            wait_bytes(buf.at[layer, pl.ds(0, 31)], sem)

        @pl.when(jnp.logical_not(fewer))
        def _():
            wait_bytes(buf.at[layer], sem)

    def send_quad(layer):
        for d in range(1, 4):
            remote(wq.at[layer, jq], wq.at[layer, jq], 3, layer, quad_partner(d)).start()

    def send_wout(layer):
        wo_loads[layer].wait()

        def body(i, carry):
            remote(wo.at[layer, h], wo.at[layer, h], 4, layer, head_partner(i)).start()
            return carry

        lax.fori_loop(1, 32, body, 0)

    def head_row(table, layer):
        row = table[layer : layer + 1, pl.ds(pl.multiple_of(lax.div(h, 2) * 128, 128), 128)]
        row = jnp.broadcast_to(row, (8, 128))
        first, second = both_halves(row, low)
        return jnp.where(h0 == 0, first, second)

    def project(layer):
        parts = []
        squares = jnp.zeros((64, 128), F32)
        for j in range(4):
            column = (j // 2) * 16 + x * 2 + j % 2
            wide = jnp.concatenate([xbuf[layer, s * 4 + j].astype(F32) for s in range(8)], axis=0)
            scale = vgain[layer : layer + 1, pl.ds(pl.multiple_of(column * 128, 128), 128)]
            parts.append((wide * scale).astype(BF16))
            squares = squares + wide * wide
        scaled = jnp.concatenate(parts, axis=1)
        wait_bytes(wq.at[layer, pl.ds(0, 3)], rsem.at[layer, 3])
        partial = jnp.dot(scaled, wq[layer].reshape(512, 384), preferred_element_type=F32)
        for s in range(8):
            pbuf[layer, s, :, 0:384] = partial[s * 8 : s * 8 + 8].astype(BF16)
            pbuf[layer, s, :, 384:512] = squares[s * 8 : s * 8 + 8].astype(BF16)
        for d in (4, 3, 5, 2, 6, 1, 7):
            to = lax.rem(x + d, 8)
            remote(pbuf.at[layer, to], rbuf.at[layer, x], 1, layer, x_partner(d)).start()
        rbuf[layer, x] = pbuf[layer, x]

    def recur(layer):
        wait_bytes(rbuf.at[layer, pl.ds(0, 7)], rsem.at[layer, 1])
        total = rbuf[layer, 0].astype(F32)
        for s in range(1, 8):
            total = total + rbuf[layer, s].astype(F32)
        mean_sq = jnp.sum(total[:, 384:512], axis=1, keepdims=True) / D
        projected = total[:, 0:384] * lax.rsqrt(mean_sq + RMS_EPS)
        r, k = both_halves(projected[:, 0:128], low)
        v, p = both_halves(projected[:, 128:256], low)
        q, g = both_halves(projected[:, 256:384], low)
        decay = jnp.exp(-math.exp(-0.5) * jax.nn.sigmoid(head_row(vbias, layer) + p))
        rate = jax.nn.sigmoid(q)
        kn = k * lax.rsqrt(jnp.sum(k * k, axis=1, keepdims=True) * 0.5 + 1.0)
        st_loads[layer].wait()
        old = jnp.stack([st[layer, :, 128 * t : 128 * t + 128] for t in range(32)])
        removed = half_sums(old * kn[None], ones)
        vs = half_sums(jnp.where(pick, v[None], 0.0), ones)
        new = old * decay[None] - removed * (kn * rate)[None] + vs * (k * rate)[None]
        for t in range(32):
            sn[layer, :, 128 * t : 128 * t + 128] = new[t]
        reads = half_sums(new * r[None], ones)
        read = jnp.sum(jnp.where(pick, reads, 0.0), axis=0)
        read = read + pltpu.roll(read, 64, 1)
        center = read - jnp.sum(read, axis=1, keepdims=True) / 128
        spread = jnp.sum(center * center, axis=1, keepdims=True) / 128
        normed = center * lax.rsqrt(spread + GROUP_EPS) * head_row(vrgain, layer)
        own = jnp.sum(r * k * head_row(vself, layer), axis=1, keepdims=True) * 0.5
        out = (normed + own * v) * jax.nn.sigmoid(g)
        osend[layer] = out.astype(BF16)

        def body(i, carry):
            dest = owner_dest(i)

            @pl.when(dest != me)
            def _():
                remote(osend.at[layer], obuf.at[layer, h], 2, layer, dest).start()

            return carry

        lax.fori_loop(0, 32, body, 0)

        @pl.when(owner_self)
        def _():
            obuf[layer, h] = osend[layer]

        pltpu.make_async_copy(sn.at[layer], new_state.at[layer, 0], lsem.at[21 + layer]).start()

    def combine(layer):
        wait_bytes(wo.at[layer, pl.ds(0, 31)], rsem.at[layer, 4])
        wait_counted(obuf, layer, rsem.at[layer, 2], owner_self)
        pieces = []
        for i in range(16):
            even = obuf[layer, 2 * i].astype(F32)
            odd = obuf[layer, 2 * i + 1].astype(F32)
            pieces.append(jnp.where(low, even, odd).astype(BF16))
        heads = jnp.concatenate(pieces, axis=1)
        branch = jnp.dot(heads, wo[layer].reshape(2048, 128), preferred_element_type=F32)
        return (xt[layer].astype(F32) + branch).astype(BF16)

    send_tiles(0)
    send_quad(0)
    send_quad(1)
    gain_load.wait()
    bias_load.wait()
    self_load.wait()
    rgain_load.wait()
    for layer in range(2):
        wait_counted(xbuf, layer, rsem.at[layer, 0], tile_self)
        send_wout(layer)
        project(layer)
        recur(layer)
        tile = combine(layer)
        if layer == 0:
            xt[1] = tile
            send_tiles(1)
        else:
            mixed[0] = tile

    for layer in range(2):
        wait_counted(xbuf, layer, ssem.at[layer, 0], tile_self)
        wait_bytes(rbuf.at[layer, pl.ds(0, 7)], ssem.at[layer, 1])
        wait_counted(obuf, layer, ssem.at[layer, 2], owner_self)
        wait_bytes(wq.at[layer, pl.ds(0, 3)], ssem.at[layer, 3])
        wait_bytes(wo.at[layer, pl.ds(0, 31)], ssem.at[layer, 4])
        pltpu.make_async_copy(sn.at[layer], new_state.at[layer, 0], lsem.at[21 + layer]).wait()


def on_device(*args):
    anywhere = pl.BlockSpec(memory_space=pl.ANY)
    return pl.pallas_call(
        kernel,
        out_shape=(
            jax.ShapeDtypeStruct((1, 8, 128), BF16),
            jax.ShapeDtypeStruct((2, 1, 8, 4096), F32),
        ),
        in_specs=[anywhere] * 13,
        out_specs=(pl.BlockSpec(memory_space=pltpu.VMEM), anywhere),
        scratch_shapes=[
            pltpu.VMEM((2, 8, 128), BF16),
            pltpu.VMEM((2, 32, 8, 128), BF16),
            pltpu.VMEM((2, 6, 128, 64), BF16),
            pltpu.VMEM((2, 4, 128, 384), BF16),
            pltpu.VMEM((2, 8, 8, 512), BF16),
            pltpu.VMEM((2, 8, 8, 512), BF16),
            pltpu.VMEM((2, 8, 128), BF16),
            pltpu.VMEM((2, 32, 8, 128), BF16),
            pltpu.VMEM((2, 32, 64, 128), BF16),
            pltpu.VMEM((2, 8, 4096), F32),
            pltpu.VMEM((2, 8, 4096), F32),
            pltpu.VMEM((2, 4096), F32),
            pltpu.VMEM((2, 2048), F32),
            pltpu.VMEM((2, 2048), F32),
            pltpu.VMEM((2, 2048), F32),
            pltpu.SemaphoreType.DMA((23,)),
            pltpu.SemaphoreType.DMA((2, 5)),
            pltpu.SemaphoreType.DMA((2, 5)),
        ],
        compiler_params=pltpu.CompilerParams(collective_id=0, has_side_effects=True),
    )(*args)


def solution(mesh):
    weight = P(None, "tp", None, None)
    return jax.shard_map(
        on_device,
        mesh=mesh,
        in_specs=(
            P("tp", None, None),
            P(),
            weight,
            weight,
            weight,
            weight,
            weight,
            weight,
            P(),
            P(),
            P(),
            weight,
            weight,
        ),
        out_specs=(P("tp", None, None), weight),
        check_vma=False,
    )
```

time: 317 us -> 88.9 us (0.28)
  the two profiles are of different devices: /device:TPU:2 before, /device:TPU:60 now
where the time goes in v1:
time: 88.9 us; the launch traced here: 88.3 us
  Pallas kernels  79.5 us (89%)
  local copies, waits for them, and re-layouts  8.17 us (9%)
    pallas_call x1, Pallas kernels, on_device(): pl.pallas_call(kernel, out_shape=(jax.ShapeDtypeStruct((1, 8, 128), BF16)...  79.5 us
    unnamed x20, local copies, waits for them, and re-layouts  8.17 us

profile of v1, /device:TPU:60, one launch (start us, length us, event | category | flops | bytes accessed | tf_op | source)
XLA Modules:
  0.0 88.3 jit_solution(14510003468960498752)
XLA Ops:
  0.6 0.0 copy-start
  0.6 1.5 %copy.15.w0 = bf16[2,1,128,64]{3,2,1,0:T(8,128)(2,1)} copy(bf16[2,1,128,64]{2,3,1,0:T(8,128)(2,1)} %param.15) | data formatting | bytes 65536 | tf_op args[2]
  2.1 0.0 copy-done
  2.1 0.0 copy-start.1
  2.1 0.7 copy.16.w1
  2.9 0.0 copy-done.1
  2.9 0.0 copy-start.2
  2.9 0.7 copy.17.w2
  3.6 0.0 copy-done.2
  3.7 0.0 copy-start.3
  3.7 0.7 copy.18.w3
  4.4 0.0 copy-done.3
  4.4 0.0 copy-start.4
  4.4 0.7 copy.19.w4
  5.2 0.0 copy-done.4
  5.2 0.7 copy.20.w5
  5.9 79.5 %shard_map.140 = (bf16[1,8,128]{2,1,0:T(8,128)(2,1)}, f32[2,1,8,4096]{3,2,1,0:T(8,128)}) custom-call(bf16[1,8,128]{2,1,0:T(8,128)(2,1)} %tokens.1, f32[2,4096]{1,0:T(2,128)} %gain.1, bf16[2,1,128,64]{3,2,1,0:T(8,128)(2,1)} %copy.15.w0, bf16[2,1,128,64]{3,2,1,0:T(8,128)(2,1)} %copy.16.w1, bf16[2,1,128,64]{3,2,1,0:T(8,128)(2,1)} %copy.17.w2, ...), custom_call_target="tpu_custom_call" | custom-call | tf_op jit(solution)/shard_map/pallas_call | solution.py:336
  85.4 0.0 copy-start.5
  85.4 0.7 copy-done.5
  86.1 0.6 copy.23
  86.6 1.7 %copy.24 = f32[2,1,8,4096]{3,2,1,0:T(8,128)} copy(f32[2,1,8,4096]{3,2,1,0:T(8,128)} %get-tuple-element.5) | data formatting | bytes 524288
Async XLA Ops:
  0.6 1.5 %copy-start = (bf16[2,1,128,64]{2,3,1,0:T(8,128)(2,1)S(1)}, bf16[2,1,128,64]{2,3,1,0:T(8,128)(2,1)}, u32[]{:S(2)}) copy-start(bf16[2,1,128,64]{2,3,1,0:T(8,128)(2,1)} %param.16) | copy-start | bytes 98308
  2.1 0.8 copy-start.1
  2.9 0.8 copy-start.2
  3.7 0.8 copy-start.3
  4.4 0.8 copy-start.4
  85.4 0.7 copy-start.5

commit v2 on v1

--- a/solution.py
+++ b/solution.py
@@ -48,7 +48,6 @@
     new_state,
     xt,
     xbuf,
-    wraw,
     wq,
     pbuf,
     rbuf,
@@ -71,6 +70,7 @@
     core = lax.rem(me, 2)
     x = lax.rem(lax.div(me, 2), 8)
     ylo = lax.rem(lax.div(me, 16), 2)
+    z = lax.div(h, 4)
     z2 = lax.div(h, 16)
     hx = lax.rem(lax.div(h, 2), 8)
     h0 = lax.rem(h, 2)
@@ -88,7 +88,7 @@
     w_loads = []
     for layer in range(2):
         for i, w in enumerate((w0, w1, w2, w3, w4, w5)):
-            w_loads.append(load(w.at[layer, 0], wraw.at[layer, i], lsem.at[1 + layer * 6 + i]))
+            w_loads.append(load(w.at[layer, 0], wq.at[layer, jq, pl.ds(64 * i, 64)], lsem.at[1 + layer * 6 + i]))
     wo_loads = [load(wout.at[l, 0], wo.at[l, h], lsem.at[13 + l]) for l in range(2)]
     gain_load = load(gain, vgain, lsem.at[15])
     bias_load = load(bias, vbias, lsem.at[16])
@@ -113,8 +113,11 @@
     def owner_dest(i):
         return b * 32 + lax.rem(lax.rem(me, 32) + 16 + i, 32)
 
-    def head_partner(i):
-        return lax.rem(h + i, 32) * 32 + b
+    def y_partner(d):
+        return (z * 4 + lax.rem(h + d, 4)) * 32 + b
+
+    def z_partner(d):
+        return lax.rem(me + d * 128, 1024)
 
     tile_self = jnp.logical_and(z2 == ylo, h0 == core)
     owner_self = h == b
@@ -136,25 +139,17 @@
         greet(x_partner(d))
     for d in range(1, 4):
         greet(quad_partner(d))
-
-    def own_weights(layer):
-        for i in range(3):
-            w_loads[layer * 6 + 2 * i].wait()
-            w_loads[layer * 6 + 2 * i + 1].wait()
-            pair = jnp.concatenate([wraw[layer, 2 * i], wraw[layer, 2 * i + 1]], axis=1)
-            wq[layer, jq, :, 128 * i : 128 * i + 128] = pair
-
-    own_weights(0)
-    own_weights(1)
+        greet(y_partner(d))
+
     tok_load.wait()
 
     @pl.when(tile_self)
     def _():
-        pl.semaphore_wait(barrier, 41)
+        pl.semaphore_wait(barrier, 44)
 
     @pl.when(jnp.logical_not(tile_self))
     def _():
-        pl.semaphore_wait(barrier, 42)
+        pl.semaphore_wait(barrier, 45)
 
     lane = lax.broadcasted_iota(jnp.int32, (8, 128), 1)
     low = lane < 64
@@ -175,23 +170,35 @@
             device_id_type=MESH,
         )
 
+    def send_all(start):
+        def first(i, carry):
+            for k in range(4):
+                start(i * 4 + k)
+            return carry
+
+        def second(i, carry):
+            for k in range(3):
+                start(17 + i * 3 + k)
+            return carry
+
+        lax.fori_loop(0, 4, first, 0)
+        lax.fori_loop(0, 5, second, 0)
+
     def send_tiles(layer):
         slot = hx * 4 + jq
 
-        def body(i, carry):
-            dest = tile_dest(i)
-
-            @pl.when(dest != me)
-            def _():
-                remote(xt.at[layer], xbuf.at[layer, slot], 0, layer, dest).start()
-
-            return carry
-
-        lax.fori_loop(0, 32, body, 0)
+        def start(i):
+            remote(xt.at[layer], xbuf.at[layer, slot], 0, layer, tile_dest(i)).start()
+
+        send_all(start)
 
         @pl.when(tile_self)
         def _():
             xbuf[layer, slot] = xt[layer]
+
+        @pl.when(jnp.logical_not(tile_self))
+        def _():
+            start(16)
 
     def wait_bytes(ref, sem):
         pltpu.make_async_copy(ref, ref, sem).wait()
@@ -206,17 +213,21 @@
             wait_bytes(buf.at[layer], sem)
 
     def send_quad(layer):
+        for i in range(6):
+            w_loads[layer * 6 + i].wait()
         for d in range(1, 4):
             remote(wq.at[layer, jq], wq.at[layer, jq], 3, layer, quad_partner(d)).start()
 
-    def send_wout(layer):
+    def send_wout_y(layer):
         wo_loads[layer].wait()
-
-        def body(i, carry):
-            remote(wo.at[layer, h], wo.at[layer, h], 4, layer, head_partner(i)).start()
-            return carry
-
-        lax.fori_loop(1, 32, body, 0)
+        for d in (2, 1, 3):
+            remote(wo.at[layer, h], wo.at[layer, h], 4, layer, y_partner(d)).start()
+
+    def send_wout_z(layer):
+        wait_bytes(wo.at[layer, pl.ds(0, 3)], rsem.at[layer, 4])
+        block = wo.at[layer, pl.ds(z * 4, 4)]
+        for d in (4, 3, 5, 2, 6, 1, 7):
+            remote(block, block, 5, layer, z_partner(d)).start()
 
     def head_row(table, layer):
         row = table[layer : layer + 1, pl.ds(pl.multiple_of(lax.div(h, 2) * 128, 128), 128)]
@@ -225,17 +236,20 @@
         return jnp.where(h0 == 0, first, second)
 
     def project(layer):
-        parts = []
+        wait_bytes(wq.at[layer, pl.ds(0, 3)], rsem.at[layer, 3])
+        partial = jnp.zeros((64, 384), F32)
         squares = jnp.zeros((64, 128), F32)
         for j in range(4):
             column = (j // 2) * 16 + x * 2 + j % 2
             wide = jnp.concatenate([xbuf[layer, s * 4 + j].astype(F32) for s in range(8)], axis=0)
             scale = vgain[layer : layer + 1, pl.ds(pl.multiple_of(column * 128, 128), 128)]
-            parts.append((wide * scale).astype(BF16))
+            partial = partial + lax.dot_general(
+                (wide * scale).astype(BF16),
+                wq[layer, j],
+                (((1,), (1,)), ((), ())),
+                preferred_element_type=F32,
+            )
             squares = squares + wide * wide
-        scaled = jnp.concatenate(parts, axis=1)
-        wait_bytes(wq.at[layer, pl.ds(0, 3)], rsem.at[layer, 3])
-        partial = jnp.dot(scaled, wq[layer].reshape(512, 384), preferred_element_type=F32)
         for s in range(8):
             pbuf[layer, s, :, 0:384] = partial[s * 8 : s * 8 + 8].astype(BF16)
             pbuf[layer, s, :, 384:512] = squares[s * 8 : s * 8 + 8].astype(BF16)
@@ -274,25 +288,23 @@
         out = (normed + own * v) * jax.nn.sigmoid(g)
         osend[layer] = out.astype(BF16)
 
-        def body(i, carry):
-            dest = owner_dest(i)
-
-            @pl.when(dest != me)
-            def _():
-                remote(osend.at[layer], obuf.at[layer, h], 2, layer, dest).start()
-
-            return carry
-
-        lax.fori_loop(0, 32, body, 0)
+        def start(i):
+            remote(osend.at[layer], obuf.at[layer, h], 2, layer, owner_dest(i)).start()
+
+        send_all(start)
 
         @pl.when(owner_self)
         def _():
             obuf[layer, h] = osend[layer]
 
+        @pl.when(jnp.logical_not(owner_self))
+        def _():
+            start(16)
+
         pltpu.make_async_copy(sn.at[layer], new_state.at[layer, 0], lsem.at[21 + layer]).start()
 
     def combine(layer):
-        wait_bytes(wo.at[layer, pl.ds(0, 31)], rsem.at[layer, 4])
+        wait_bytes(wo.at[layer, pl.ds(0, 28)], rsem.at[layer, 5])
         wait_counted(obuf, layer, rsem.at[layer, 2], owner_self)
         pieces = []
         for i in range(16):
@@ -301,23 +313,28 @@
             pieces.append(jnp.where(low, even, odd).astype(BF16))
         heads = jnp.concatenate(pieces, axis=1)
         branch = jnp.dot(heads, wo[layer].reshape(2048, 128), preferred_element_type=F32)
-        return (xt[layer].astype(F32) + branch).astype(BF16)
+        return xt[layer].astype(F32) + branch
 
     send_tiles(0)
     send_quad(0)
-    send_quad(1)
+    send_wout_y(0)
+    send_wout_y(1)
     gain_load.wait()
     bias_load.wait()
     self_load.wait()
     rgain_load.wait()
     for layer in range(2):
         wait_counted(xbuf, layer, rsem.at[layer, 0], tile_self)
-        send_wout(layer)
+        if layer == 1:
+            send_wout_z(1)
         project(layer)
+        if layer == 0:
+            send_wout_z(0)
+            send_quad(1)
         recur(layer)
         tile = combine(layer)
         if layer == 0:
-            xt[1] = tile
+            xt[1] = tile.astype(BF16)
             send_tiles(1)
         else:
             mixed[0] = tile
@@ -327,16 +344,18 @@
         wait_bytes(rbuf.at[layer, pl.ds(0, 7)], ssem.at[layer, 1])
         wait_counted(obuf, layer, ssem.at[layer, 2], owner_self)
         wait_bytes(wq.at[layer, pl.ds(0, 3)], ssem.at[layer, 3])
-        wait_bytes(wo.at[layer, pl.ds(0, 31)], ssem.at[layer, 4])
+        wait_bytes(wo.at[layer, pl.ds(0, 3)], ssem.at[layer, 4])
+        wait_bytes(wo.at[layer, pl.ds(0, 28)], ssem.at[layer, 5])
         pltpu.make_async_copy(sn.at[layer], new_state.at[layer, 0], lsem.at[21 + layer]).wait()
 
 
 def on_device(*args):
+    args = args[:2] + tuple(jnp.swapaxes(w, 2, 3) for w in args[2:8]) + args[8:]
     anywhere = pl.BlockSpec(memory_space=pl.ANY)
-    return pl.pallas_call(
+    mixed, new_state = pl.pallas_call(
         kernel,
         out_shape=(
-            jax.ShapeDtypeStruct((1, 8, 128), BF16),
+            jax.ShapeDtypeStruct((1, 8, 128), F32),
             jax.ShapeDtypeStruct((2, 1, 8, 4096), F32),
         ),
         in_specs=[anywhere] * 13,
@@ -344,8 +363,7 @@
         scratch_shapes=[
             pltpu.VMEM((2, 8, 128), BF16),
             pltpu.VMEM((2, 32, 8, 128), BF16),
-            pltpu.VMEM((2, 6, 128, 64), BF16),
-            pltpu.VMEM((2, 4, 128, 384), BF16),
+            pltpu.VMEM((2, 4, 384, 128), BF16),
             pltpu.VMEM((2, 8, 8, 512), BF16),
             pltpu.VMEM((2, 8, 8, 512), BF16),
             pltpu.VMEM((2, 8, 128), BF16),
@@ -358,11 +376,12 @@
             pltpu.VMEM((2, 2048), F32),
             pltpu.VMEM((2, 2048), F32),
             pltpu.SemaphoreType.DMA((23,)),
-            pltpu.SemaphoreType.DMA((2, 5)),
-            pltpu.SemaphoreType.DMA((2, 5)),
+            pltpu.SemaphoreType.DMA((2, 6)),
+            pltpu.SemaphoreType.DMA((2, 6)),
         ],
         compiler_params=pltpu.CompilerParams(collective_id=0, has_side_effects=True),
     )(*args)
+    return mixed.astype(BF16), new_state
 
 
 def solution(mesh):

time: 88.9 us -> 75.9 us (0.85)
  the two profiles are of different devices: /device:TPU:60 before, /device:TPU:1 now
where the time goes in v2:
time: 75.9 us; the launch traced here: 75.7 us
  Pallas kernels  72.1 us (95%)
  local copies, waits for them, and re-layouts  1.67 us (2%)
  other arithmetic  1.26 us (2%)
    pallas_call x1, Pallas kernels, on_device(): pl.pallas_call(kernel, out_shape=(jax.ShapeDtypeStruct((1, 8, 128), F32),...  72.1 us
    unnamed x1, local copies, waits for them, and re-layouts  1.67 us

profile of v2, /device:TPU:1, one launch (start us, length us, event | category | flops | bytes accessed | tf_op | source)
XLA Modules:
  0.0 75.7 jit_solution(3282774396532274894)
XLA Ops:
  0.6 72.1 %shard_map.140 = (f32[1,8,128]{2,1,0:T(8,128)}, f32[2,1,8,4096]{3,2,1,0:T(8,128)}) custom-call(bf16[1,8,128]{2,1,0:T(8,128)(2,1)} %tokens.1, f32[2,4096]{1,0:T(2,128)} %gain.1, bf16[2,1,64,128]{3,2,1,0:T(8,128)(2,1)} %bitcast.6, bf16[2,1,64,128]{3,2,1,0:T(8,128)(2,1)} %bitcast.7, bf16[2,1,64,128]{3,2,1,0:T(8,128)(2,1)} %bitcast.8, ...), custom_call_target="tpu_custom_call" | custom-call | tf_op jit(solution)/shard_map/pallas_call | solution.py:355
  72.7 1.3 %convert_element_type.3 = bf16[1,8,128]{2,1,0:T(8,128)(2,1)} convert(f32[1,8,128]{2,1,0:T(8,128)} %get-tuple-element.4) | non-fusion elementwise | flops 1024 | bytes 6144 | tf_op jit(solution)/shard_map/convert_element_type | solution.py:384
  74.0 1.7 %copy.16 = f32[2,1,8,4096]{3,2,1,0:T(8,128)} copy(f32[2,1,8,4096]{3,2,1,0:T(8,128)} %get-tuple-element.9) | data formatting | bytes 524288

commit v3 on v2

--- a/solution.py
+++ b/solution.py
@@ -85,6 +85,59 @@
         return copy
 
     tok_load = load(tokens.at[0], xt.at[0], lsem.at[0])
+
+    def tile_dest(i):
+        other = lax.rem(h + 16 + i, 32)
+        return other * 32 + z2 * 16 + x * 2 + h0
+
+    def tile_source(i):
+        tile_head = ylo * 16 + lax.rem(lax.div(i, 4) + hx, 8) * 2 + core
+        quad = lax.rem(i + jq, 4)
+        return tile_head * 32 + lax.div(quad, 2) * 16 + x * 2 + lax.rem(quad, 2)
+
+    def x_partner(d):
+        return me - x * 2 + lax.rem(x + d, 8) * 2
+
+    def quad_partner(d):
+        other = lax.rem(jq + d, 4)
+        return me - ylo * 16 - core + lax.div(other, 2) * 16 + lax.rem(other, 2)
+
+    def owner_dest(i):
+        return b * 32 + lax.rem(lax.rem(me, 32) + 16 + i, 32)
+
+    def y_partner(d):
+        return (z * 4 + lax.rem(h + d, 4)) * 32 + b
+
+    def z_partner(d):
+        return lax.rem(me + d * 128, 1024)
+
+    tile_self = jnp.logical_and(z2 == ylo, h0 == core)
+    owner_self = h == b
+
+    barrier = pltpu.get_barrier_semaphore()
+
+    def greet(device):
+        pl.semaphore_signal(barrier, inc=1, device_id=(device,), device_id_type=MESH)
+
+    def greet_sources(i, carry):
+        for k in range(4):
+            greet(tile_source(i * 4 + k))
+        return carry
+
+    lax.fori_loop(1, 8, greet_sources, 0)
+    for i in range(1, 4):
+        greet(tile_source(i))
+
+    @pl.when(jnp.logical_not(tile_self))
+    def _():
+        greet(tile_source(0))
+
+    for d in range(1, 8):
+        greet(x_partner(d))
+    for d in range(1, 4):
+        greet(quad_partner(d))
+        greet(y_partner(d))
+
     w_loads = []
     for layer in range(2):
         for i, w in enumerate((w0, w1, w2, w3, w4, w5)):
@@ -95,51 +148,6 @@
     self_load = load(selfw, vself, lsem.at[17])
     rgain_load = load(rgain, vrgain, lsem.at[18])
     st_loads = [load(state.at[l, 0], st.at[l], lsem.at[19 + l]) for l in range(2)]
-
-    def tile_dest(i):
-        other = lax.rem(h + 16 + i, 32)
-        return other * 32 + z2 * 16 + x * 2 + h0
-
-    def tile_source(i):
-        return (ylo * 16 + lax.div(i, 4) * 2 + core) * 32 + lax.div(lax.rem(i, 4), 2) * 16 + x * 2 + lax.rem(i, 2)
-
-    def x_partner(d):
-        return me - x * 2 + lax.rem(x + d, 8) * 2
-
-    def quad_partner(d):
-        other = lax.rem(jq + d, 4)
-        return me - ylo * 16 - core + lax.div(other, 2) * 16 + lax.rem(other, 2)
-
-    def owner_dest(i):
-        return b * 32 + lax.rem(lax.rem(me, 32) + 16 + i, 32)
-
-    def y_partner(d):
-        return (z * 4 + lax.rem(h + d, 4)) * 32 + b
-
-    def z_partner(d):
-        return lax.rem(me + d * 128, 1024)
-
-    tile_self = jnp.logical_and(z2 == ylo, h0 == core)
-    owner_self = h == b
-
-    barrier = pltpu.get_barrier_semaphore()
-
-    def greet(device):
-        pl.semaphore_signal(barrier, inc=1, device_id=(device,), device_id_type=MESH)
-
-    def greet_source(i, carry):
-        @pl.when(tile_source(i) != me)
-        def _():
-            greet(tile_source(i))
-
-        return carry
-
-    lax.fori_loop(0, 32, greet_source, 0)
-    for d in range(1, 8):
-        greet(x_partner(d))
-    for d in range(1, 4):
-        greet(quad_partner(d))
-        greet(y_partner(d))
 
     tok_load.wait()
 
@@ -318,7 +326,6 @@
     send_tiles(0)
     send_quad(0)
     send_wout_y(0)
-    send_wout_y(1)
     gain_load.wait()
     bias_load.wait()
     self_load.wait()
@@ -331,6 +338,7 @@
         if layer == 0:
             send_wout_z(0)
             send_quad(1)
+            send_wout_y(1)
         recur(layer)
         tile = combine(layer)
         if layer == 0:

time: 75.9 us -> 75.2 us (level)
  no operation moved by 1% of the time
where the time goes in v3:
time: 75.2 us; the launch traced here: 75 us
  Pallas kernels  71.4 us (95%)
  local copies, waits for them, and re-layouts  1.67 us (2%)
  other arithmetic  1.26 us (2%)
    pallas_call x1, Pallas kernels, on_device(): pl.pallas_call(kernel, out_shape=(jax.ShapeDtypeStruct((1, 8, 128), F32),...  71.4 us
    unnamed x1, local copies, waits for them, and re-layouts  1.67 us

profile of v3, /device:TPU:1, one launch (start us, length us, event | category | flops | bytes accessed | tf_op | source)
XLA Modules:
  0.0 75.0 jit_solution(13599220301747186472)
XLA Ops:
  0.6 71.4 %shard_map.140 = (f32[1,8,128]{2,1,0:T(8,128)}, f32[2,1,8,4096]{3,2,1,0:T(8,128)}) custom-call(bf16[1,8,128]{2,1,0:T(8,128)(2,1)} %tokens.1, f32[2,4096]{1,0:T(2,128)} %gain.1, bf16[2,1,64,128]{3,2,1,0:T(8,128)(2,1)} %bitcast.6, bf16[2,1,64,128]{3,2,1,0:T(8,128)(2,1)} %bitcast.7, bf16[2,1,64,128]{3,2,1,0:T(8,128)(2,1)} %bitcast.8, ...), custom_call_target="tpu_custom_call" | custom-call | tf_op jit(solution)/shard_map/pallas_call | solution.py:363
  72.1 1.3 %convert_element_type.3 = bf16[1,8,128]{2,1,0:T(8,128)(2,1)} convert(f32[1,8,128]{2,1,0:T(8,128)} %get-tuple-element.4) | non-fusion elementwise | flops 1024 | bytes 6144 | tf_op jit(solution)/shard_map/convert_element_type | solution.py:392
  73.3 1.7 %copy.16 = f32[2,1,8,4096]{3,2,1,0:T(8,128)} copy(f32[2,1,8,4096]{3,2,1,0:T(8,128)} %get-tuple-element.9) | data formatting | bytes 524288
